TPU v7x, 32 devices: a whole 2x2x4 slice. The times are simulated.
32 devices in a mesh: grp: 2 (over y), fs: 4 (over z), tp: 4 (over x, core).
Axes of the slice: x: 2, y: 2, z: 4, core: 2. Of those that a mesh axis runs over, the one named last changes fastest.
Arguments:
- tokens: bfloat16 [1792, 2048], P(('grp', 'fs'), 'tp'), parts along dimension 0, may hold values from -6 to 6
- route_ids: int32 [1792, 2], P(('grp', 'fs')), parts along dimension 0, may hold values from 0 to 3, all different within a row; in each aligned block of 224 rows (0 to 223, 224 to 447, ...) at most 168 rows name the same one
- route_weights: float32 [1792, 2], P(('grp', 'fs')), parts along dimension 0, may hold values from 0.25 to 1
- norm_gain: float32 [2048], P('fs'), may hold values from 0.1 to 1.9
- gate_master: float32 [4, 2048, 512], P(None, 'fs', 'tp'), may hold values from -0.125 to 0.125
- up_master: float32 [4, 2048, 512], P(None, 'fs', 'tp'), may hold values from -0.125 to 0.125
- down_master: float32 [4, 2048, 512], P(None, 'fs', 'tp'), may hold values from -0.25 to 0.25
Outputs:
- gate_serve: bfloat16 [8, 2048, 512], P(('grp', 'fs'), None, 'tp'), parts along dimension 0
- up_serve: bfloat16 [8, 2048, 512], P(('grp', 'fs'), None, 'tp'), parts along dimension 0
- down_serve: bfloat16 [8, 2048, 512], P(('grp', 'fs'), None, 'tp'), parts along dimension 0
- moe_output: bfloat16 [1792, 2048], P(('grp', 'fs'), 'tp'), parts along dimension 0
There are 2 independent parts, one for each index of `grp`. A program takes and returns all parts, laid end to end along the dimension named above; an argument that names none is the same for every part. Nothing has to cross between parts.
Inputs may be any that keep to these rules, and one draw needn't show every extreme that they name: `route_ids`: the 2 experts of a row differ; within the rows of one index of fs (aligned blocks of 224 rows) no expert is named more than 168 times.
All inputs are finite; a program needn't handle non-finite values.
Results may differ from a plain program's by a relative error of at most 0.012.
Values may be sent and summed in bfloat16 or wider, within the bound.
A program may use at most 64 MiB of HBM per device.

v0:
```python
import jax
import jax.numpy as jnp
from jax import lax
from jax.sharding import PartitionSpec as P

norm_epsilon = 1e-06


def slot_numbers(route_ids, experts, capacity):
    flat_ids = route_ids.reshape(-1)
    onehot = (flat_ids[:, None] == jnp.arange(experts, dtype=jnp.int32)[None, :]).astype(jnp.int32)
    before = jnp.cumsum(onehot, axis=0) - onehot
    position = jnp.sum(before * onehot, axis=1)
    return (flat_ids * capacity + position).reshape(route_ids.shape)


def local(tokens, route_ids, route_weights, norm_gain, gate_master, up_master, down_master):
    experts = gate_master.shape[0]
    shards = lax.axis_size("fs")
    columns = lax.axis_size("tp")
    per_device = experts // shards
    tok_rows = route_ids.shape[0]
    top_count = route_ids.shape[1]
    local_width = tokens.shape[1]
    model_width = local_width * columns
    capacity = max(2, 3 * tok_rows * top_count // (2 * experts))
    row_gain = norm_gain[None, :, None]
    gate_half = (gate_master * row_gain).astype(jnp.bfloat16)
    up_half = (up_master * row_gain).astype(jnp.bfloat16)
    down_half = down_master.astype(jnp.bfloat16)
    gate_serve, up_serve, down_serve = (
        lax.all_to_all(gate_half, "fs", split_axis=0, concat_axis=1, tiled=True),
        lax.all_to_all(up_half, "fs", split_axis=0, concat_axis=1, tiled=True),
        lax.all_to_all(down_half, "fs", split_axis=0, concat_axis=1, tiled=True),
    )
    slot_ids = slot_numbers(route_ids, experts, capacity)
    slot_range = jnp.arange(experts * capacity, dtype=jnp.int32)
    selects = [
        (slot_ids[:, rank_slot, None] == slot_range[None, :]).astype(jnp.bfloat16)
        for rank_slot in range(top_count)
    ]
    placing = selects[0]
    for extra in selects[1:]:
        placing = placing + extra
    local_values = tokens.astype(jnp.float32)
    squares = lax.psum(jnp.sum(local_values * local_values, axis=1), "tp")
    inverse = lax.rsqrt(squares / model_width + norm_epsilon)[:, None]
    normed = (local_values * inverse).astype(jnp.bfloat16)
    buffer = jnp.einsum("ts,td->sd", placing, normed, preferred_element_type=jnp.float32).astype(
        jnp.bfloat16
    )
    arrived = lax.all_to_all(
        buffer.reshape(shards, per_device * capacity, local_width),
        "fs",
        split_axis=0,
        concat_axis=0,
        tiled=True,
    )
    arrived = arrived.reshape(shards, per_device, capacity, local_width)
    partial_value = lax.all_gather(arrived, "tp", axis=3, tiled=True)
    gate_sum = jnp.einsum(
        "sxcd,xdf->xscf", partial_value, gate_serve, preferred_element_type=jnp.float32
    )
    up_sum = jnp.einsum(
        "sxcd,xdf->xscf", partial_value, up_serve, preferred_element_type=jnp.float32
    )
    hidden = (jax.nn.silu(gate_sum) * up_sum).astype(jnp.bfloat16)
    products = jnp.einsum("xdf,xscf->dsxc", down_serve, hidden, preferred_element_type=jnp.float32)
    summed = lax.psum_scatter(
        products.reshape(local_width * lax.axis_size("tp"), shards * per_device * capacity).astype(
            jnp.bfloat16
        ),
        "tp",
        scatter_dimension=0,
        tiled=True,
    )
    returned = lax.all_to_all(
        summed.reshape(local_width, shards, per_device * capacity),
        "fs",
        split_axis=1,
        concat_axis=1,
        tiled=True,
    )
    returned = returned.reshape(local_width, experts * capacity)
    combined = jnp.zeros((tok_rows, local_width), jnp.float32)
    for rank_slot in range(top_count):
        picked = jnp.einsum(
            "ts,ds->td", selects[rank_slot], returned, preferred_element_type=jnp.float32
        )
        combined = combined + route_weights[:, rank_slot : rank_slot + 1] * picked
    return (gate_serve, up_serve, down_serve, combined.astype(jnp.bfloat16))


def solution(mesh):
    placed = (
        P(("grp", "fs"), "tp"),
        P(("grp", "fs"), None),
        P(("grp", "fs"), None),
        P("fs"),
        P(None, "fs", "tp"),
        P(None, "fs", "tp"),
        P(None, "fs", "tp"),
    )
    return jax.shard_map(
        local,
        mesh=mesh,
        in_specs=placed,
        out_specs=(
            P(("grp", "fs"), None, "tp"),
            P(("grp", "fs"), None, "tp"),
            P(("grp", "fs"), None, "tp"),
            P(("grp", "fs"), "tp"),
        ),
        check_vma=False,
    )
```

profile of v0, /device:TPU:0, one launch (start us, length us, event | category | flops | bytes accessed | tf_op | source)
XLA Modules:
  0.0 170.7 jit_solution(8881094231520576288)
XLA Ops:
  7.2 0.0 copy-start.7
  7.2 0.0 copy-start.5
  7.2 0.0 copy-start.4
  7.2 0.0 all-gather.3.cloned.1.call-start
  7.2 0.9 copy.17
  8.2 0.1 eq.52
  8.4 1.2 reduce-window.6
  9.6 0.2 slice_reduce_fusion
  9.8 0.2 reduce-window.9
  10.0 0.1 add_bitcast_fusion
  10.1 0.1 reduce_sum.21
  10.3 0.1 copy.18
  10.3 0.7 multiply_add_fusion
  11.0 1.1 fusion.5
  12.1 8.4 %psum.7 = f32[224]{0:T(256)S(1)} all-reduce(f32[224]{0:T(256)S(1)} %fusion.5), channel_id=1, replica_groups=mesh['grp'=2,'fs'=4,'tp'=4] {'tp'}, use_global_device_ids=true, to_apply=%region_4.5 | all-reduce | flops 224 | bytes 1792 | tf_op jit(solution)/shard_map/psum | solution.py:46
  20.5 1.5 convolution_convert_fusion.1
  22.0 21.6 %all_to_all.46 = bf16[4,168,512]{2,1,0:T(8,128)(2,1)} all-to-all(bf16[4,168,512]{2,1,0:T(8,128)(2,1)S(1)} %bitcast.48), channel_id=1, replica_groups=mesh['grp'=2,'fs'=4,'tp'=4] {'fs'}, dimensions={0} | all-to-all | bytes 1376256 | tf_op jit(solution)/shard_map/all_to_all | solution.py:52
  43.5 0.0 all-gather.3.cloned.1.call-update
  43.6 0.0 copy-done.7
  43.6 0.0 copy-done.5
  43.6 0.0 copy-done.4
  43.6 0.0 copy-start.3
  43.6 1.0 multiply_convert_fusion
  44.6 16.2 %all_to_all.47 = bf16[4,512,128]{2,1,0:T(8,128)(2,1)S(1)} all-to-all(bf16[4,512,128]{2,1,0:T(8,128)(2,1)S(1)} %get-tuple-element.9), channel_id=1, replica_groups=mesh['grp'=2,'fs'=4,'tp'=4] {'fs'}, dimensions={0} | all-to-all | bytes 1048576 | tf_op jit(solution)/shard_map/all_to_all | solution.py:32
  60.9 3.5 %all-to-all-start.1 = ((bf16[4,512,128]{2,1,0:T(8,128)(2,1)}), bf16[4,512,128]{2,1,0:T(8,128)(2,1)S(1)}, u32[]{:S(2)}, u32[]{:S(2)}) async-start(bf16[4,512,128]{2,1,0:T(8,128)(2,1)} %get-tuple-element.8), calls=%async_computation.1 | async-start | bytes 1048576 | tf_op jit(solution)/shard_map/all_to_all | solution.py:33
  64.4 0.0 copy-done.3
  64.4 0.9 convert_element_type.49
  65.2 12.6 %all-to-all-done.1 = bf16[4,512,128]{2,1,0:T(8,128)(2,1)S(1)} async-done(((bf16[4,512,128]{2,1,0:T(8,128)(2,1)}), bf16[4,512,128]{2,1,0:T(8,128)(2,1)S(1)}, u32[]{:S(2)}, u32[]{:S(2)}) %all-to-all-start.1) | async-done | bytes 524320 | tf_op jit(solution)/shard_map/all_to_all | solution.py:33
  77.9 4.1 %all-to-all-start.2 = ((bf16[4,512,128]{2,1,0:T(8,128)(2,1)}), bf16[4,512,128]{2,1,0:T(8,128)(2,1)}, u32[]{:S(2)}, u32[]{:S(2)}) async-start(bf16[4,512,128]{2,1,0:T(8,128)(2,1)} %convert_element_type.49), calls=%async_computation.2 | async-start | bytes 1048576 | tf_op jit(solution)/shard_map/all_to_all | solution.py:34
  82.0 0.0 reduce-scatter.2.cloned.1.call-start
  82.1 0.0 copy-done.1
  82.1 0.0 all-gather.3.cloned.1.call-done
  82.1 0.0 copy-start
  82.1 3.5 %fusion.27 = f32[4,168,128]{2,1,0:T(8,128)} fusion(bf16[4,168,2048]{2,1,0:T(8,128)(2,1)} %all-gather.3.cloned.1.call-done, bf16[2048,128,1]{1,0,2:T(8,128)(2,1)S(1)} %bitcast.41), kind=kOutput, calls=%fused_computation.44 | convolution fusion | flops 352321536 | bytes 3620864 | tf_op jit(solution)/shard_map/sxcd,xdf->xscf/dot_general | solution.py:61
  85.7 10.5 %all-to-all-done.2 = bf16[4,512,128]{2,1,0:T(8,128)(2,1)} async-done(((bf16[4,512,128]{2,1,0:T(8,128)(2,1)}), bf16[4,512,128]{2,1,0:T(8,128)(2,1)}, u32[]{:S(2)}, u32[]{:S(2)}) %all-to-all-start.2) | async-done | bytes 524320 | tf_op jit(solution)/shard_map/all_to_all | solution.py:34
  96.1 0.0 copy-done
  96.1 5.8 %convolution_convert_fusion = bf16[4,168,2048]{2,1,0:T(8,128)(2,1)} fusion(bf16[2048,128,1]{1,0,2:T(8,128)(2,1)} %bitcast.13, bf16[4,168,2048]{2,1,0:T(8,128)(2,1)S(1)} %copy-done, bf16[2048,128,1]{1,0,2:T(8,128)(2,1)} %bitcast.43, f32[4,168,128]{2,1,0:T(8,128)} %fusion.27), kind=kOutput, calls=%fused_computation | convolution fusion | flops 706535424 | bytes 6897664 | tf_op jit(solution)/shard_map/xdf,xscf->dsxc/dot_general | solution.py:68
  102.0 0.0 reduce-scatter.2.cloned.1.call-update
  102.0 0.0 copy-start.2
  102.0 34.5 %reduce-scatter.2.cloned.1.call-done = bf16[512,672]{0,1:T(8,128)(2,1)} async-done(((bf16[2048,672]{0,1:T(8,128)(2,1)}), bf16[512,672]{0,1:T(8,128)(2,1)}) %reduce-scatter.2.cloned.1.call-update) | async-done | bytes 688144 | tf_op jit(solution)/shard_map/reduce_scatter | solution.py:69
  136.5 4.6 %all-to-all-start.4 = ((bf16[512,4,168]{0,2,1:T(8,128)(2,1)}), bf16[512,4,168]{0,2,1:T(8,128)(2,1)S(1)}, u32[]{:S(2)}, u32[]{:S(2)}) async-start(bf16[512,4,168]{0,2,1:T(8,128)(2,1)} %bitcast.47), calls=%async_computation.5 | async-start | bytes 1376256 | tf_op jit(solution)/shard_map/all_to_all | solution.py:77
  141.1 0.0 copy-done.6
  141.1 17.8 %all-to-all-done.4 = bf16[512,4,168]{0,2,1:T(8,128)(2,1)S(1)} async-done(((bf16[512,4,168]{0,2,1:T(8,128)(2,1)}), bf16[512,4,168]{0,2,1:T(8,128)(2,1)S(1)}, u32[]{:S(2)}, u32[]{:S(2)}) %all-to-all-start.4) | async-done | bytes 688160 | tf_op jit(solution)/shard_map/all_to_all | solution.py:77
  158.9 0.4 convolution_multiply_fusion.1
  159.3 1.1 fusion.1
  160.4 0.8 copy.25
  161.2 0.8 copy.26
  162.0 1.9 %copy.27 = bf16[1,2048,128]{2,1,0:T(8,128)(2,1)} copy(bf16[1,2048,128]{2,1,0:T(8,128)(2,1)} %bitcast.2) | data formatting | bytes 1048576
  (11 shorter events, 0.1 us)
Async XLA Ops:
  7.2 36.4 %copy-start.7 = (f32[512]{0:T(512)S(1)}, f32[512]{0:T(512)}, u32[]{:S(2)}) copy-start(f32[512]{0:T(512)} %param.10) | copy-start | bytes 6148
  7.2 36.4 %copy-start.5 = (f32[4,512,128]{2,1,0:T(8,128)S(1)}, f32[4,512,128]{2,1,0:T(8,128)}, u32[]{:S(2)}) copy-start(f32[4,512,128]{2,1,0:T(8,128)} %param.11) | copy-start | bytes 3145732
  7.2 36.4 %copy-start.4 = (f32[4,512,128]{2,1,0:T(8,128)S(1)}, f32[4,512,128]{2,1,0:T(8,128)}, u32[]{:S(2)}) copy-start(f32[4,512,128]{2,1,0:T(8,128)} %param.12) | copy-start | bytes 3145732
  7.2 74.9 %all-gather.3.cloned.1.call-start = ((), (), s32[]{:S(2)}) async-start(), calls=%async_computation.7 | async-start | bytes 3440640 | tf_op jit(solution)/shard_map/all_gather | solution.py:60
  43.6 20.8 %copy-start.3 = (f32[4,512,128]{2,1,0:T(8,128)S(1)}, f32[4,512,128]{2,1,0:T(8,128)}, u32[]{:S(2)}) copy-start(f32[4,512,128]{2,1,0:T(8,128)} %param.13) | copy-start | bytes 3145732
  60.9 17.0 %all-to-all-start.1 = ((bf16[4,512,128]{2,1,0:T(8,128)(2,1)}), bf16[4,512,128]{2,1,0:T(8,128)(2,1)S(1)}, u32[]{:S(2)}, u32[]{:S(2)}) async-start(bf16[4,512,128]{2,1,0:T(8,128)(2,1)} %get-tuple-element.8), calls=%async_computation.1 | async-start | bytes 1048576 | tf_op jit(solution)/shard_map/all_to_all | solution.py:33
  77.9 4.2 %copy-start.1 = (bf16[4,512,128]{2,1,0:T(8,128)(2,1)}, bf16[4,512,128]{2,1,0:T(8,128)(2,1)S(1)}, u32[]{:S(2)}) copy-start(bf16[4,512,128]{2,1,0:T(8,128)(2,1)S(1)} %all-to-all-done.1) | copy-start | bytes 1572868
  77.9 18.3 %all-to-all-start.2 = ((bf16[4,512,128]{2,1,0:T(8,128)(2,1)}), bf16[4,512,128]{2,1,0:T(8,128)(2,1)}, u32[]{:S(2)}, u32[]{:S(2)}) async-start(bf16[4,512,128]{2,1,0:T(8,128)(2,1)} %convert_element_type.49), calls=%async_computation.2 | async-start | bytes 1048576 | tf_op jit(solution)/shard_map/all_to_all | solution.py:34
  82.0 54.5 %reduce-scatter.2.cloned.1.call-start = ((), (), s32[]{:S(2)}) async-start(), calls=%async_computation.6 | async-start | bytes 3440640 | tf_op jit(solution)/shard_map/reduce_scatter | solution.py:69
  82.1 14.0 %copy-start = (bf16[4,168,2048]{2,1,0:T(8,128)(2,1)S(1)}, bf16[4,168,2048]{2,1,0:T(8,128)(2,1)}, u32[]{:S(2)}) copy-start(bf16[4,168,2048]{2,1,0:T(8,128)(2,1)} %all-gather.3.cloned.1.call-done) | copy-start | bytes 8257540
  102.0 39.1 %copy-start.6 = (f32[224,2]{0,1:T(2,128)S(1)}, f32[224,2]{0,1:T(2,128)}, u32[]{:S(2)}) copy-start(f32[224,2]{0,1:T(2,128)} %param.9) | copy-start | bytes 5380
  102.0 59.2 %copy-start.2 = (bf16[4,512,128]{2,1,0:T(8,128)(2,1)S(1)}, bf16[4,512,128]{2,1,0:T(8,128)(2,1)}, u32[]{:S(2)}) copy-start(bf16[4,512,128]{2,1,0:T(8,128)(2,1)} %copy-done.1) | copy-start | bytes 1572868
  136.5 22.4 %all-to-all-start.4 = ((bf16[512,4,168]{0,2,1:T(8,128)(2,1)}), bf16[512,4,168]{0,2,1:T(8,128)(2,1)S(1)}, u32[]{:S(2)}, u32[]{:S(2)}) async-start(bf16[512,4,168]{0,2,1:T(8,128)(2,1)} %bitcast.47), calls=%async_computation.5 | async-start | bytes 1376256 | tf_op jit(solution)/shard_map/all_to_all | solution.py:77
Sparse Core Ops, SparseCore 0:
  43.7 25.4 all-gather.2
  102.1 34.3 reduce-scatter.1
where the time goes:
time: 171 us
  waiting for transfers between devices  75.5 us (44%)
  blocking collectives  46.2 us (27%)
  between operations  14.2 us (8%)
  starting transfers between devices  12.3 us (7%)
  matrix products  12.3 us (7%)
  other arithmetic  5.18 us (3%)
  local copies, waits for them, and re-layouts  5.04 us (3%)
    reduce_scatter x1, waiting for transfers between devices, local(): lax.psum_scatter(products.reshape(local_width * lax.axis_size('tp'), shar...  34.5 us
    all_to_all x1, blocking collectives, local(): lax.all_to_all(buffer.reshape(shards, per_device * capacity, local_width)...  21.6 us
    all_to_all x1, waiting for transfers between devices, local(): lax.all_to_all(summed.reshape(local_width, shards, per_device * capacity)...  17.8 us
    all_to_all x1, blocking collectives, local(): lax.all_to_all(gate_half, 'fs', split_axis=0, concat_axis=1, tiled=True)  16.2 us
    all_to_all x1, waiting for transfers between devices, local(): lax.all_to_all(up_half, 'fs', split_axis=0, concat_axis=1, tiled=True)  12.6 us
    all_to_all x1, waiting for transfers between devices, local(): lax.all_to_all(down_half, 'fs', split_axis=0, concat_axis=1, tiled=True)  10.5 us
    psum x1, blocking collectives, local(): squares = lax.psum(jnp.sum(local_values * local_values, axis=1), 'tp')  8.37 us
    dot_general x1, matrix products, local(): jnp.einsum('xdf,xscf->dsxc', down_serve, hidden, preferred_element_type=j...  5.82 us
  transfers between devices with their start and end apart: 5, of which 4 were waited for; matrix products, arithmetic and copies ran while one was open for 3% of the time, Pallas kernels for 0%

commit v1 on v0

--- a/solution.py
+++ b/solution.py
@@ -49,13 +49,19 @@
     buffer = jnp.einsum("ts,td->sd", placing, normed, preferred_element_type=jnp.float32).astype(
         jnp.bfloat16
     )
-    arrived = lax.all_to_all(
-        buffer.reshape(shards, per_device * capacity, local_width),
-        "fs",
-        split_axis=0,
-        concat_axis=0,
-        tiled=True,
-    )
+    shard = buffer.reshape(shards, per_device * capacity, local_width)
+    ways, here = (lax.axis_size("fs"), lax.axis_index("fs"))
+    width = shard.shape[0] // ways
+    shape = list(shard.shape)
+    shape[0] = width
+    height = shape[0]
+    shape[0] = height * ways
+    arrived = jnp.zeros(shape, shard.dtype)
+    for mask in range(ways):
+        part = lax.dynamic_slice_in_dim(shard, (here ^ mask) * width, width, axis=0)
+        if mask:
+            part = lax.ppermute(part, "fs", [(d, d ^ mask) for d in range(ways)])
+        arrived = lax.dynamic_update_slice_in_dim(arrived, part, (here ^ mask) * height, axis=0)
     arrived = arrived.reshape(shards, per_device, capacity, local_width)
     partial_value = lax.all_gather(arrived, "tp", axis=3, tiled=True)
     gate_sum = jnp.einsum(

time: 171 us -> 171 us (level)
  blocking collectives: 46.2 us -> 24.9 us
  waiting for transfers between devices: 75.5 us -> 87.2 us
  starting transfers between devices: 12.3 us -> 16.7 us
  local copies, waits for them, and re-layouts: 5.04 us -> 9.43 us
    all_to_all x2 -> x1, blocking collectives: 37.8 us -> 16.6 us  [local(): lax.all_to_all(up_half, 'fs', split_axis=0, concat_axis=1, tiled=True)]
    ppermute x0 -> x3, waiting for transfers between devices: none -> 11.2 us  [local(): part = lax.ppermute(part, 'fs', [(d, d ^ mask) for d in range(ways)])]
    ppermute x0 -> x3, starting transfers between devices: none -> 4.39 us  [local(): part = lax.ppermute(part, 'fs', [(d, d ^ mask) for d in range(ways)])]
    dynamic_update_slice x0 -> x4, local copies, waits for them, and re-layouts: none -> 2.82 us  [local(): lax.dynamic_update_slice_in_dim(arrived, part, (here ^ mask) * height, ax...]
    unnamed x21 -> x23, local copies, waits for them, and re-layouts: 4.44 us -> 5.15 us
  transfers between devices with their start and end apart: 5 -> 8, of which waited for: 4 -> 6; matrix products, arithmetic and copies ran while one was open for 3% -> 4% of each run, Pallas kernels for 0% -> 0%
where the time goes in v1:
time: 171 us; the launch traced here: 170 us
  waiting for transfers between devices  87.2 us (51%)
  blocking collectives  24.9 us (15%)
  starting transfers between devices  16.7 us (10%)
  between operations  14.3 us (8%)
  matrix products  12.3 us (7%)
  local copies, waits for them, and re-layouts  9.43 us (6%)
  other arithmetic  5.33 us (3%)
    reduce_scatter x1, waiting for transfers between devices, local(): lax.psum_scatter(products.reshape(local_width * lax.axis_size('tp'), shar...  35.2 us
    all_to_all x1, waiting for transfers between devices, local(): lax.all_to_all(summed.reshape(local_width, shards, per_device * capacity)...  17.8 us
    all_to_all x1, blocking collectives, local(): lax.all_to_all(up_half, 'fs', split_axis=0, concat_axis=1, tiled=True)  16.6 us
    all_to_all x1, waiting for transfers between devices, local(): lax.all_to_all(gate_half, 'fs', split_axis=0, concat_axis=1, tiled=True)  12.5 us
    ppermute x3, waiting for transfers between devices, local(): part = lax.ppermute(part, 'fs', [(d, d ^ mask) for d in range(ways)])  11.2 us
    all_to_all x1, waiting for transfers between devices, local(): lax.all_to_all(down_half, 'fs', split_axis=0, concat_axis=1, tiled=True)  10.4 us
    psum x1, blocking collectives, local(): squares = lax.psum(jnp.sum(local_values * local_values, axis=1), 'tp')  8.37 us
    dot_general x1, matrix products, local(): jnp.einsum('xdf,xscf->dsxc', down_serve, hidden, preferred_element_type=j...  5.81 us
  transfers between devices with their start and end apart: 8, of which 6 were waited for; matrix products, arithmetic and copies ran while one was open for 4% of the time, Pallas kernels for 0%

profile of v1, /device:TPU:0, one launch (start us, length us, event | category | flops | bytes accessed | tf_op | source)
XLA Modules:
  0.0 170.1 jit_solution(16203623944920428865)
XLA Ops:
  7.2 0.0 all-gather.2.cloned.1.call-start
  7.2 0.8 copy.23
  8.0 0.1 eq.52
  8.2 1.2 reduce-window.6
  9.4 0.2 slice_reduce_fusion
  9.7 0.2 reduce-window.9
  9.8 0.1 add_bitcast_fusion
  10.0 0.1 reduce_sum.21
  10.1 0.1 copy.24
  10.2 0.7 multiply_add_fusion
  10.9 0.0 copy-start.8
  10.9 1.2 fusion.8
  12.1 8.4 %psum.7 = f32[224]{0:T(256)S(1)} all-reduce(f32[224]{0:T(256)S(1)} %fusion.8), channel_id=1, replica_groups=mesh['grp'=2,'fs'=4,'tp'=4] {'tp'}, use_global_device_ids=true, to_apply=%region_4.5 | all-reduce | flops 224 | bytes 1792 | tf_op jit(solution)/shard_map/psum | solution.py:46
  20.5 1.5 convolution_convert_fusion.1
  22.0 0.8 constant_dynamic-slice_fusion
  22.8 1.6 collective-permute-start
  24.4 2.6 %collective-permute-start.1 = (bf16[1,168,512]{2,1,0:T(8,128)(2,1)}, bf16[1,168,512]{2,1,0:T(8,128)(2,1)}, u32[]{:S(2)}, u32[]{:S(2)}) collective-permute-start(bf16[1,168,512]{2,1,0:T(8,128)(2,1)} %get-tuple-element.5), channel_id=1, source_target_pairs={{0,8},{4,12},{8,0},{12,4},{1,9},{5,13},{9,1},{13,5},{2,10},{6,14},... | collective-permute-start | bytes 516104 | tf_op jit(solution)/shard_map/ppermute | solution.py:63
  27.0 0.2 collective-permute-start.2
  27.2 3.3 %collective-permute-done = bf16[1,168,512]{2,1,0:T(8,128)(2,1)} collective-permute-done((bf16[1,168,512]{2,1,0:T(8,128)(2,1)}, bf16[1,168,512]{2,1,0:T(8,128)(2,1)}, u32[]{:S(2)}, u32[]{:S(2)}) %collective-permute-start) | collective-permute-done | bytes 172064 | tf_op jit(solution)/shard_map/ppermute | solution.py:63
  30.6 0.9 bitcast_dynamic-update-slice_fusion.1
  31.5 7.9 %collective-permute-done.1 = bf16[1,168,512]{2,1,0:T(8,128)(2,1)} collective-permute-done((bf16[1,168,512]{2,1,0:T(8,128)(2,1)}, bf16[1,168,512]{2,1,0:T(8,128)(2,1)}, u32[]{:S(2)}, u32[]{:S(2)}) %collective-permute-start.1) | collective-permute-done | bytes 172064 | tf_op jit(solution)/shard_map/ppermute | solution.py:63
  39.4 0.9 bitcast_dynamic-update-slice_fusion
  40.4 0.0 collective-permute-done.2
  40.4 0.9 bitcast_dynamic-update-slice_fusion.2
  41.3 0.9 copy-done.3
  42.2 0.0 all-gather.2.cloned.1.call-update
  42.2 0.0 copy-start.4
  42.2 1.0 multiply_convert_fusion
  43.3 16.6 %all_to_all.41 = bf16[4,512,128]{2,1,0:T(8,128)(2,1)S(1)} all-to-all(bf16[4,512,128]{2,1,0:T(8,128)(2,1)S(1)} %get-tuple-element.11), channel_id=1, replica_groups=mesh['grp'=2,'fs'=4,'tp'=4] {'fs'}, dimensions={0} | all-to-all | bytes 1048576 | tf_op jit(solution)/shard_map/all_to_all | solution.py:33
  59.8 3.5 %all-to-all-start = ((bf16[4,512,128]{2,1,0:T(8,128)(2,1)}), bf16[4,512,128]{2,1,0:T(8,128)(2,1)S(1)}, u32[]{:S(2)}, u32[]{:S(2)}) async-start(bf16[4,512,128]{2,1,0:T(8,128)(2,1)} %get-tuple-element.12), calls=%async_computation | async-start | bytes 1048576 | tf_op jit(solution)/shard_map/all_to_all | solution.py:32
  63.3 0.9 convert_element_type.49
  64.2 12.5 %all-to-all-done = bf16[4,512,128]{2,1,0:T(8,128)(2,1)S(1)} async-done(((bf16[4,512,128]{2,1,0:T(8,128)(2,1)}), bf16[4,512,128]{2,1,0:T(8,128)(2,1)S(1)}, u32[]{:S(2)}, u32[]{:S(2)}) %all-to-all-start) | async-done | bytes 524320 | tf_op jit(solution)/shard_map/all_to_all | solution.py:32
  76.7 4.1 %all-to-all-start.2 = ((bf16[4,512,128]{2,1,0:T(8,128)(2,1)}), bf16[4,512,128]{2,1,0:T(8,128)(2,1)}, u32[]{:S(2)}, u32[]{:S(2)}) async-start(bf16[4,512,128]{2,1,0:T(8,128)(2,1)} %convert_element_type.49), calls=%async_computation.2 | async-start | bytes 1048576 | tf_op jit(solution)/shard_map/all_to_all | solution.py:34
  80.9 0.0 reduce-scatter.2.cloned.1.call-start
  80.9 0.0 copy-done.1
  80.9 0.0 all-gather.2.cloned.1.call-done
  81.0 3.5 %fusion = f32[4,168,128]{2,1,0:T(8,128)} fusion(bf16[2048,128,1]{1,0,2:T(8,128)(2,1)S(1)} %bitcast.60, bf16[4,1,168,2048]{3,2,0,1:T(8,128)(2,1)} %all-gather.2.cloned.1.call-done), kind=kOutput, calls=%fused_computation.1 | convolution fusion | flops 352321536 | bytes 3620864 | tf_op jit(solution)/shard_map/sxcd,xdf->xscf/dot_general | solution.py:70
  84.5 10.4 %all-to-all-done.2 = bf16[4,512,128]{2,1,0:T(8,128)(2,1)} async-done(((bf16[4,512,128]{2,1,0:T(8,128)(2,1)}), bf16[4,512,128]{2,1,0:T(8,128)(2,1)}, u32[]{:S(2)}, u32[]{:S(2)}) %all-to-all-start.2) | async-done | bytes 524320 | tf_op jit(solution)/shard_map/all_to_all | solution.py:34
  94.9 5.8 %convolution_convert_fusion = bf16[4,168,2048]{2,1,0:T(8,128)(2,1)} fusion(bf16[2048,128,1]{1,0,2:T(8,128)(2,1)} %bitcast.20, f32[4,168,128]{2,1,0:T(8,128)} %fusion, bf16[2048,128,1]{1,0,2:T(8,128)(2,1)} %bitcast.62, bf16[4,1,168,2048]{3,2,0,1:T(8,128)(2,1)S(1)} %copy-done), kind=kOutput, calls=%fused_computation | convolution fusion | flops 706535424 | bytes 6897664 | tf_op jit(solution)/shard_map/xdf,xscf->dsxc/dot_general | solution.py:74
  100.7 0.0 reduce-scatter.2.cloned.1.call-update
  100.8 35.2 %reduce-scatter.2.cloned.1.call-done = bf16[512,672]{0,1:T(8,128)(2,1)} async-done(((bf16[2048,672]{0,1:T(8,128)(2,1)}), bf16[512,672]{0,1:T(8,128)(2,1)}) %reduce-scatter.2.cloned.1.call-update) | async-done | bytes 688144 | tf_op jit(solution)/shard_map/reduce_scatter | solution.py:75
  135.9 4.6 %all-to-all-start.3 = ((bf16[512,4,168]{0,2,1:T(8,128)(2,1)}), bf16[512,4,168]{0,2,1:T(8,128)(2,1)S(1)}, u32[]{:S(2)}, u32[]{:S(2)}) async-start(bf16[512,4,168]{0,2,1:T(8,128)(2,1)} %bitcast.66), calls=%async_computation.4 | async-start | bytes 1376256 | tf_op jit(solution)/shard_map/all_to_all | solution.py:83
  140.5 17.8 %all-to-all-done.3 = bf16[512,4,168]{0,2,1:T(8,128)(2,1)S(1)} async-done(((bf16[512,4,168]{0,2,1:T(8,128)(2,1)}), bf16[512,4,168]{0,2,1:T(8,128)(2,1)S(1)}, u32[]{:S(2)}, u32[]{:S(2)}) %all-to-all-start.3) | async-done | bytes 688160 | tf_op jit(solution)/shard_map/all_to_all | solution.py:83
  158.4 0.4 convolution_multiply_fusion.1
  158.8 1.1 fusion.5
  159.8 0.8 copy.37
  160.6 0.8 copy.38
  161.4 1.9 %copy.39 = bf16[1,2048,128]{2,1,0:T(8,128)(2,1)} copy(bf16[1,2048,128]{2,1,0:T(8,128)(2,1)} %bitcast.2) | data formatting | bytes 1048576
  (24 shorter events, 0.2 us)
Async XLA Ops:
  7.2 73.8 %all-gather.2.cloned.1.call-start = ((), (), s32[]{:S(2)}) async-start(), calls=%async_computation.5 | async-start | bytes 3440640 | tf_op jit(solution)/shard_map/all_gather | solution.py:66
  10.9 31.3 %copy-start.5 = (f32[4,512,128]{2,1,0:T(8,128)S(1)}, f32[4,512,128]{2,1,0:T(8,128)}, u32[]{:S(2)}) copy-start(f32[4,512,128]{2,1,0:T(8,128)} %param.12) | copy-start | bytes 3145732
  10.9 31.3 %copy-start.6 = (f32[4,512,128]{2,1,0:T(8,128)S(1)}, f32[4,512,128]{2,1,0:T(8,128)}, u32[]{:S(2)}) copy-start(f32[4,512,128]{2,1,0:T(8,128)} %param.11) | copy-start | bytes 3145732
  10.9 31.3 %copy-start.8 = (f32[512]{0:T(512)S(1)}, f32[512]{0:T(512)}, u32[]{:S(2)}) copy-start(f32[512]{0:T(512)} %param.10) | copy-start | bytes 6148
  22.8 7.8 %collective-permute-start = (bf16[1,168,512]{2,1,0:T(8,128)(2,1)}, bf16[1,168,512]{2,1,0:T(8,128)(2,1)}, u32[]{:S(2)}, u32[]{:S(2)}) collective-permute-start(bf16[1,168,512]{2,1,0:T(8,128)(2,1)} %get-tuple-element.6), channel_id=1, source_target_pairs={{0,4},{4,0},{8,12},{12,8},{1,5},{5,1},{9,13},{13,9},{2,6},{6,2},{1... | collective-permute-start | bytes 516104 | tf_op jit(solution)/shard_map/ppermute | solution.py:63
  24.4 15.1 %collective-permute-start.1 = (bf16[1,168,512]{2,1,0:T(8,128)(2,1)}, bf16[1,168,512]{2,1,0:T(8,128)(2,1)}, u32[]{:S(2)}, u32[]{:S(2)}) collective-permute-start(bf16[1,168,512]{2,1,0:T(8,128)(2,1)} %get-tuple-element.5), channel_id=1, source_target_pairs={{0,8},{4,12},{8,0},{12,4},{1,9},{5,13},{9,1},{13,5},{2,10},{6,14},... | collective-permute-start | bytes 516104 | tf_op jit(solution)/shard_map/ppermute | solution.py:63
  27.0 13.4 %collective-permute-start.2 = (bf16[1,168,512]{2,1,0:T(8,128)(2,1)}, bf16[1,168,512]{2,1,0:T(8,128)(2,1)}, u32[]{:S(2)}, u32[]{:S(2)}) collective-permute-start(bf16[1,168,512]{2,1,0:T(8,128)(2,1)} %get-tuple-element.4), channel_id=1, source_target_pairs={{0,12},{4,8},{8,4},{12,0},{1,13},{5,9},{9,5},{13,1},{2,14},{6,10},... | collective-permute-start | bytes 516104 | tf_op jit(solution)/shard_map/ppermute | solution.py:63
  41.3 0.9 copy-start.3
  42.2 21.1 %copy-start.4 = (f32[4,512,128]{2,1,0:T(8,128)S(1)}, f32[4,512,128]{2,1,0:T(8,128)}, u32[]{:S(2)}) copy-start(f32[4,512,128]{2,1,0:T(8,128)} %param.13) | copy-start | bytes 3145732
  59.8 16.9 %all-to-all-start = ((bf16[4,512,128]{2,1,0:T(8,128)(2,1)}), bf16[4,512,128]{2,1,0:T(8,128)(2,1)S(1)}, u32[]{:S(2)}, u32[]{:S(2)}) async-start(bf16[4,512,128]{2,1,0:T(8,128)(2,1)} %get-tuple-element.12), calls=%async_computation | async-start | bytes 1048576 | tf_op jit(solution)/shard_map/all_to_all | solution.py:32
  76.7 4.2 %copy-start.1 = (bf16[4,512,128]{2,1,0:T(8,128)(2,1)}, bf16[4,512,128]{2,1,0:T(8,128)(2,1)S(1)}, u32[]{:S(2)}) copy-start(bf16[4,512,128]{2,1,0:T(8,128)(2,1)S(1)} %all-to-all-done) | copy-start | bytes 1572868
  76.7 18.2 %all-to-all-start.2 = ((bf16[4,512,128]{2,1,0:T(8,128)(2,1)}), bf16[4,512,128]{2,1,0:T(8,128)(2,1)}, u32[]{:S(2)}, u32[]{:S(2)}) async-start(bf16[4,512,128]{2,1,0:T(8,128)(2,1)} %convert_element_type.49), calls=%async_computation.2 | async-start | bytes 1048576 | tf_op jit(solution)/shard_map/all_to_all | solution.py:34
  80.9 55.0 %reduce-scatter.2.cloned.1.call-start = ((), (), s32[]{:S(2)}) async-start(), calls=%async_computation.6 | async-start | bytes 3440640 | tf_op jit(solution)/shard_map/reduce_scatter | solution.py:75
  81.0 14.0 %copy-start = (bf16[4,1,168,2048]{3,2,0,1:T(8,128)(2,1)S(1)}, bf16[4,1,168,2048]{3,2,0,1:T(8,128)(2,1)}, u32[]{:S(2)}) copy-start(bf16[4,1,168,2048]{3,2,0,1:T(8,128)(2,1)} %all-gather.2.cloned.1.call-done) | copy-start | bytes 8257540
  100.7 39.8 %copy-start.7 = (f32[224,2]{0,1:T(2,128)S(1)}, f32[224,2]{0,1:T(2,128)}, u32[]{:S(2)}) copy-start(f32[224,2]{0,1:T(2,128)} %param.9) | copy-start | bytes 5380
  100.7 59.1 %copy-start.2 = (bf16[4,512,128]{2,1,0:T(8,128)(2,1)S(1)}, bf16[4,512,128]{2,1,0:T(8,128)(2,1)}, u32[]{:S(2)}) copy-start(bf16[4,512,128]{2,1,0:T(8,128)(2,1)} %copy-done.1) | copy-start | bytes 1572868
  135.9 22.4 %all-to-all-start.3 = ((bf16[512,4,168]{0,2,1:T(8,128)(2,1)}), bf16[512,4,168]{0,2,1:T(8,128)(2,1)S(1)}, u32[]{:S(2)}, u32[]{:S(2)}) async-start(bf16[512,4,168]{0,2,1:T(8,128)(2,1)} %bitcast.66), calls=%async_computation.4 | async-start | bytes 1376256 | tf_op jit(solution)/shard_map/all_to_all | solution.py:83
Sparse Core Ops, SparseCore 0:
  42.3 26.4 all-gather.1
  100.9 34.9 reduce-scatter.1
